TPU v7x, 32 devices: a whole 2x2x4 slice. The times are simulated.
32 devices in a mesh: kv: 4 (over y, x), tp: 8 (over z, core).
Axes of the slice: x: 2, y: 2, z: 4, core: 2. Of those that a mesh axis runs over, the one named last changes fastest.
Arguments:
- tokens: bfloat16 [64, 4096], P(None, ('kv', 'tp')), may hold values from -6 to 6
- memory: float32 [64, 16, 256, 128], P('kv', 'tp'), may hold values from -6 to 6
- normalizer: float32 [64, 16, 128], P('kv', 'tp'), may hold values from -6 to 6
- stabilizer: float32 [64, 16], P('kv', 'tp'), may hold values from -4 to 4
- first_gain: float32 [4096], replicated, may hold values from 0.1 to 1.9
- first_gate: bfloat16 [4096, 12288], P('kv', 'tp'), may hold values from -0.09375 to 0.09375
- first_up: bfloat16 [4096, 12288], P('kv', 'tp'), may hold values from -0.09375 to 0.09375
- first_down: bfloat16 [12288, 4096], P('tp', 'kv'), may hold values from -0.078125 to 0.078125
- mixer_gain: float32 [4096], replicated, may hold values from 0.1 to 1.9
- query_weight: bfloat16 [4096, 2048], P(None, 'tp'), may hold values from -0.09375 to 0.09375
- key_weight: bfloat16 [4096, 2048], P(None, 'tp'), may hold values from -0.09375 to 0.09375
- value_weight: bfloat16 [4096, 4096], P(None, 'tp'), may hold values from -0.09375 to 0.09375
- input_weight: bfloat16 [4096, 16], replicated, may hold values from -0.09375 to 0.09375
- forget_weight: bfloat16 [4096, 16], replicated, may hold values from -0.09375 to 0.09375
- forget_bias: float32 [16], P('tp'), may hold values from -2 to 4
- output_weight: bfloat16 [4096, 4096], P('tp'), may hold values from -0.09375 to 0.09375
- last_gain: float32 [4096], replicated, may hold values from 0.1 to 1.9
- last_gate: bfloat16 [4096, 12288], P('kv', 'tp'), may hold values from -0.09375 to 0.09375
- last_up: bfloat16 [4096, 12288], P('kv', 'tp'), may hold values from -0.09375 to 0.09375
- last_down: bfloat16 [12288, 4096], P('tp', 'kv'), may hold values from -0.078125 to 0.078125
Outputs:
- result: bfloat16 [64, 4096], P(None, ('kv', 'tp'))
- new_memory: float32 [64, 16, 256, 128], P('kv', 'tp')
- new_normalizer: float32 [64, 16, 128], P('kv', 'tp')
- new_stabilizer: float32 [64, 16], P('kv', 'tp')
All inputs are finite; a program needn't handle non-finite values.
Results may differ from a plain program's by a relative error of at most 0.025.
Values may be sent and summed in bfloat16 or wider, within the bound.
A program may use at most 128 MiB of HBM per device.

v0:
```python
import jax
import jax.numpy as jnp
from jax import lax
from jax.sharding import PartitionSpec as P

EPS = 1e-06


def hidden_units(gate_acc, up_acc, squares, model_width):
    scale = lax.rsqrt(squares / model_width + EPS)[:, None]
    return (jax.nn.silu(scale * gate_acc) * (scale * up_acc)).astype(jnp.bfloat16)


def gated_block(block, gain, w_gate, w_up, w_down, model_width):
    f32 = jnp.float32
    width = block.shape[1]
    gain_block = lax.dynamic_slice_in_dim(gain, lax.axis_index("kv") * width, width, 0)
    values = block.astype(f32)
    scaled = (values * gain_block).astype(jnp.bfloat16)
    gate_part = jnp.dot(scaled, w_gate, preferred_element_type=f32)
    up_part = jnp.dot(scaled, w_up, preferred_element_type=f32)
    squares = jnp.sum(values * values, axis=1)
    gate_acc, up_acc, sq_total = (
        lax.psum(gate_part.astype(jnp.bfloat16), "kv").astype(jnp.float32),
        lax.psum(up_part.astype(jnp.bfloat16), "kv").astype(jnp.float32),
        lax.psum(squares.astype(jnp.bfloat16), "kv").astype(jnp.float32),
    )
    hidden = hidden_units(gate_acc, up_acc, sq_total, model_width)
    share = lax.psum_scatter(
        lax.dot_general(
            w_down, hidden, (((0,), (1,)), ((), ())), preferred_element_type=f32
        ).astype(jnp.bfloat16),
        "tp",
        scatter_dimension=0,
        tiled=True,
    ).astype(jnp.float32)
    return share.T


def body(
    tokens,
    memory,
    normalizer,
    stabilizer,
    first_gain,
    first_gate,
    first_up,
    first_down,
    mixer_gain,
    query_weight,
    key_weight,
    value_weight,
    input_weight,
    forget_weight,
    forget_bias,
    output_weight,
    last_gain,
    last_gate,
    last_up,
    last_down,
):
    f32 = jnp.float32
    model_width = first_gain.shape[0]
    rows, col_width = tokens.shape
    block = lax.all_gather(tokens, "tp", axis=1, tiled=True)
    first_share = gated_block(block, first_gain, first_gate, first_up, first_down, model_width)
    stream_one = (tokens.astype(f32) + 0.5 * first_share).astype(jnp.bfloat16)
    seq_count, head_count, value_size, key_size = memory.shape
    moved = lax.all_to_all(
        stream_one.reshape(rows, 1, col_width), "kv", split_axis=0, concat_axis=1, tiled=True
    )
    own_rows = lax.all_gather(moved, "tp", axis=2, tiled=True).reshape(seq_count, model_width)
    row_values = own_rows.astype(f32)
    scale = lax.rsqrt(jnp.mean(row_values * row_values, axis=1, keepdims=True) + EPS)
    cell_in = (row_values * mixer_gain).astype(jnp.bfloat16)
    query = (
        scale * jnp.dot(cell_in, query_weight, preferred_element_type=f32) * key_size ** (-0.5)
    ).reshape(seq_count, head_count, key_size)
    key = (scale * jnp.dot(cell_in, key_weight, preferred_element_type=f32)).reshape(
        seq_count, head_count, key_size
    )
    value = (scale * jnp.dot(cell_in, value_weight, preferred_element_type=f32)).reshape(
        seq_count, head_count, value_size
    )
    first_head = lax.axis_index("tp") * head_count
    input_all = scale * jnp.dot(cell_in, input_weight, preferred_element_type=f32)
    forget_all = scale * jnp.dot(cell_in, forget_weight, preferred_element_type=f32)
    input_pre = lax.dynamic_slice_in_dim(input_all, first_head, head_count, 1)
    log_forget = jax.nn.log_sigmoid(
        lax.dynamic_slice_in_dim(forget_all, first_head, head_count, 1) + forget_bias
    )
    carried = log_forget + stabilizer
    new_stabilizer = jnp.maximum(carried, input_pre)
    keep = jnp.exp(carried - new_stabilizer)
    admit = jnp.exp(input_pre - new_stabilizer)
    recalled = jnp.einsum("bhvd,bhd->bhv", memory, query, precision=lax.Precision.HIGHEST)
    match = jnp.sum(query * key, axis=-1)
    numer = keep[..., None] * recalled + (admit * match)[..., None] * value
    denom = keep * jnp.sum(normalizer * query, axis=-1) + admit * match
    cell_out = (
        (numer / jnp.maximum(jnp.abs(denom), 1.0)[..., None])
        .reshape(seq_count, head_count * value_size)
        .astype(jnp.bfloat16)
    )
    new_memory = (
        keep[..., None, None] * memory
        + admit[..., None, None] * value[..., :, None] * key[..., None, :]
    )
    new_normalizer = keep[..., None] * normalizer + admit[..., None] * key
    partial_heads = jnp.dot(cell_out, output_weight, preferred_element_type=f32)
    mixed = lax.psum(partial_heads.astype(jnp.bfloat16), "tp").astype(jnp.float32)
    rows_two = (row_values + mixed).astype(jnp.bfloat16)
    whole_two = lax.all_to_all(rows_two, "kv", split_axis=1, concat_axis=0, tiled=True)
    last_share = gated_block(whole_two, last_gain, last_gate, last_up, last_down, model_width)
    own_columns = lax.dynamic_slice_in_dim(
        whole_two, lax.axis_index("tp") * col_width, col_width, 1
    )
    result = (own_columns.astype(f32) + 0.5 * last_share).astype(jnp.bfloat16)
    return (result, new_memory, new_normalizer, new_stabilizer)


def solution(mesh):
    in_specs = (
        P(None, ("kv", "tp")),
        P("kv", "tp", None, None),
        P("kv", "tp", None),
        P("kv", "tp"),
        P(),
        P("kv", "tp"),
        P("kv", "tp"),
        P("tp", "kv"),
        P(),
        P(None, "tp"),
        P(None, "tp"),
        P(None, "tp"),
        P(),
        P(),
        P("tp"),
        P("tp", None),
        P(),
        P("kv", "tp"),
        P("kv", "tp"),
        P("tp", "kv"),
    )
    out_specs = (
        P(None, ("kv", "tp")),
        P("kv", "tp", None, None),
        P("kv", "tp", None),
        P("kv", "tp"),
    )
    return jax.shard_map(body, mesh=mesh, in_specs=in_specs, out_specs=out_specs, check_vma=False)
```

profile of v0, /device:TPU:0, one launch (start us, length us, event | category | flops | bytes accessed | tf_op | source)
XLA Modules:
  0.0 307.5 jit_solution(12249599025583255382)
XLA Ops:
  7.2 14.9 %all_gather.6 = bf16[64,1024]{1,0:T(8,128)(2,1)S(1)} all-gather(bf16[64,128]{1,0:T(8,128)(2,1)} %param.20), channel_id=1, replica_groups=mesh['kv'=4,'tp'=8] {'tp'}, dimensions={1}, use_global_device_ids=true | all-gather | bytes 147456 | tf_op jit(solution)/shard_map/all_gather | solution.py:65
  22.1 0.8 dynamic_slice.15
  23.0 1.3 convolution_convert_fusion.3
  24.3 1.3 convolution_convert_fusion.4
  25.8 10.0 %psum.49 = bf16[64]{0:T(256)(128)(2,1)S(1)} all-reduce(bf16[64]{0:T(256)(128)(2,1)S(1)} %fusion.3), channel_id=1, replica_groups=mesh['kv'=4,'tp'=8] {'kv'}, use_global_device_ids=true, to_apply=%region_1.0 | all-reduce | flops 64 | bytes 256 | tf_op jit(solution)/shard_map/psum | solution.py:26
  35.8 34.0 %all-reduce.10.cloned.1.call-done = (bf16[64,1536]{1,0:T(8,128)(2,1)}, bf16[64,1536]{1,0:T(8,128)(2,1)}) async-done(((bf16[64,1536]{1,0:T(8,128)(2,1)}, bf16[64,1536]{1,0:T(8,128)(2,1)}), (bf16[64,1536]{1,0:T(8,128)(2,1)}, bf16[64,1536]{1,0:T(8,128)(2,1)})) %all-reduce.10.cloned.1.call-update) | async-done | bytes 393232 | tf_op jit(solution)/shard_map/psum | solution.py:25
  69.8 2.8 fusion
  72.6 0.8 copy.87
  73.5 30.9 %reduce-scatter.7.cloned.1.call-done = bf16[128,64]{1,0:T(8,128)(2,1)} async-done(((bf16[1024,64]{1,0:T(8,128)(2,1)}), bf16[128,64]{1,0:T(8,128)(2,1)}) %reduce-scatter.7.cloned.1.call-update) | async-done | bytes 16400
  104.4 0.8 copy.88
  105.8 0.7 reduce.3
  106.5 0.6 reshape.77
  107.1 3.7 %all-to-all-start = ((bf16[4,2,1024]{2,1,0:T(2,128)(2,1)}), bf16[4,2,1024]{2,1,0:T(2,128)(2,1)S(1)}, u32[]{:S(2)}, u32[]{:S(2)}) async-start(bf16[4,2,1024]{2,1,0:T(2,128)(2,1)} %reshape.77), calls=%async_computation | async-start | bytes 32768 | tf_op jit(solution)/shard_map/all_to_all | solution.py:69
  110.8 4.7 %all-to-all-done = bf16[4,2,1024]{2,1,0:T(2,128)(2,1)S(1)} async-done(((bf16[4,2,1024]{2,1,0:T(2,128)(2,1)}), bf16[4,2,1024]{2,1,0:T(2,128)(2,1)S(1)}, u32[]{:S(2)}, u32[]{:S(2)}) %all-to-all-start) | async-done | bytes 16416 | tf_op jit(solution)/shard_map/all_to_all | solution.py:69
  115.5 12.8 %all-gather = bf16[16,4,1,1024]{3,0,1,2:T(8,128)(2,1)S(1)} all-gather(bf16[16,4,1,128]{3,0,1,2:T(8,128)(2,1)S(1)} %bitcast.73), channel_id=2, replica_groups=mesh['kv'=4,'tp'=8] {'tp'}, dimensions={3}, use_global_device_ids=true | all-gather | bytes 147456 | tf_op jit(solution)/shard_map/all_gather | solution.py:72
  128.8 0.5 copy-done.8
  129.4 1.9 fusion.2
  131.3 0.7 reshape.61
  132.0 0.6 reshape.70
  132.6 3.5 %convolution_multiply_fusion = f32[16,512]{1,0:T(8,128)} fusion(bf16[16,4096]{1,0:T(8,128)(2,1)S(1)} %multiply_convert_fusion.3, bf16[4096,512]{1,0:T(8,128)(2,1)} %param.31, f32[16]{0:T(128)} %copy-done.8), kind=kOutput, calls=%fused_computation.10 | convolution fusion | flops 67117056 | bytes 4358208 | tf_op jit(solution)/shard_map/dot_general | solution.py:82
  136.0 1.4 reshape.63
  137.4 2.6 convolution_multiply_fusion.1
  140.0 0.7 reshape.62
  140.7 1.4 multiply_reduce_fusion.2
  142.2 1.3 copy.76
  143.5 1.3 copy.74
  144.8 1.1 fusion.26
  145.9 1.1 fusion.25
  147.0 1.4 abs_maximum_fusion
  148.7 5.8 %fusion.27 = f32[16,2,1,256]{3,2,1,0:T(1,128)S(1)} fusion(f32[16,2,128,1]{2,3,1,0:T(1,128)} %bitcast.71, f32[16,2,256,128]{3,2,1,0:T(8,128)} %param.21), kind=kOutput, calls=%fused_computation.61 | convolution fusion | flops 12582912 | bytes 4243456 | tf_op jit(solution)/shard_map/bhvd,bhd->bhv/dot_general | solution.py:96
  154.7 1.3 convolution_convert_fusion
  156.1 51.8 %all-reduce.6.cloned.1.call-done = bf16[16,4096]{1,0:T(8,128)(2,1)} async-done(((bf16[16,4096]{1,0:T(8,128)(2,1)}), bf16[16,4096]{1,0:T(8,128)(2,1)}) %all-reduce.6.cloned.1.call-update) | async-done | bytes 131088 | tf_op jit(solution)/shard_map/psum | solution.py:111
  207.9 0.9 add_convert_fusion
  208.8 0.7 copy.100
  209.5 3.6 %all-to-all-start.1 = ((bf16[16,4,1024]{2,0,1:T(8,128)(2,1)}), bf16[16,4,1024]{2,0,1:T(8,128)(2,1)S(1)}, u32[]{:S(2)}, u32[]{:S(2)}) async-start(bf16[16,4,1024]{2,0,1:T(8,128)(2,1)} %bitcast.63), calls=%async_computation.1 | async-start | bytes 262144 | tf_op jit(solution)/shard_map/all_to_all | solution.py:113
  213.1 0.7 dynamic_slice.19
  213.8 4.3 %all-to-all-done.1 = bf16[16,4,1024]{2,0,1:T(8,128)(2,1)S(1)} async-done(((bf16[16,4,1024]{2,0,1:T(8,128)(2,1)}), bf16[16,4,1024]{2,0,1:T(8,128)(2,1)S(1)}, u32[]{:S(2)}, u32[]{:S(2)}) %all-to-all-start.1) | async-done | bytes 131104 | tf_op jit(solution)/shard_map/all_to_all | solution.py:113
  218.2 3.4 %convolution_convert_fusion.1 = bf16[64,1536]{1,0:T(8,128)(2,1)} fusion(bf16[1024,1536]{1,0:T(8,128)(2,1)} %param.38, bf16[64,1024]{1,0:T(8,128)(2,1)S(1)} %bitcast.66, f32[1024]{0:T(1024)S(1)} %dynamic_slice.19), kind=kOutput, calls=%fused_computation.2 | convolution fusion | flops 201621504 | bytes 3477504 | tf_op jit(solution)/shard_map/dot_general | solution.py:21
  221.5 1.3 convolution_convert_fusion.2
  223.1 8.5 %psum.53 = bf16[64]{0:T(256)(128)(2,1)S(1)} all-reduce(bf16[64]{0:T(256)(128)(2,1)S(1)} %convert_element_type.143), channel_id=1, replica_groups=mesh['kv'=4,'tp'=8] {'kv'}, use_global_device_ids=true, to_apply=%region_10.11 | all-reduce | flops 64 | bytes 256 | tf_op jit(solution)/shard_map/psum | solution.py:26
  231.6 33.2 %all-reduce.8.cloned.1.call-done = (bf16[64,1536]{1,0:T(8,128)(2,1)}, bf16[64,1536]{1,0:T(8,128)(2,1)}) async-done(((bf16[64,1536]{1,0:T(8,128)(2,1)}, bf16[64,1536]{1,0:T(8,128)(2,1)}), (bf16[64,1536]{1,0:T(8,128)(2,1)}, bf16[64,1536]{1,0:T(8,128)(2,1)})) %all-reduce.8.cloned.1.call-update) | async-done | bytes 393232 | tf_op jit(solution)/shard_map/psum | solution.py:25
  264.8 2.8 fusion.1
  267.6 0.8 copy.89
  268.5 4.2 %multiply_add_fusion = f32[16,2,256,128]{3,2,1,0:T(8,128)} fusion(f32[16,2,256,128]{3,2,1,0:T(8,128)} %param.21, f32[16,2,128]{2,1,0:T(2,128)S(1)} %reshape.62, f32[16,2,256]{2,1,0:T(2,128)S(1)} %get-tuple-element.15, f32[16,2]{1,0:T(8,128)S(1)} %copy.73), kind=kLoop, calls=%fused_computation.1 | loop fusion | flops 3145728 | bytes 8437888 | tf_op jit(solution)/shard_map/add | solution.py:106
  272.7 0.7 multiply_add_fusion.1
  273.5 26.0 %reduce-scatter.9.cloned.1.call-done = bf16[128,64]{1,0:T(8,128)(2,1)} async-done(((bf16[1024,64]{1,0:T(8,128)(2,1)}), bf16[128,64]{1,0:T(8,128)(2,1)}) %reduce-scatter.9.cloned.1.call-update) | async-done | bytes 16400
  299.5 0.8 copy.90
  300.3 0.6 fusion.11
  (49 shorter events, 2.1 us)
Async XLA Ops:
  7.2 15.8 %copy-start = (bf16[1024,1536]{1,0:T(8,128)(2,1)S(1)}, bf16[1024,1536]{1,0:T(8,128)(2,1)}, u32[]{:S(2)}) copy-start(bf16[1024,1536]{1,0:T(8,128)(2,1)} %param.26) | copy-start | bytes 9437188
  7.2 62.6 %all-reduce.10.cloned.1.call-start = ((), (), s32[]{:S(2)}) async-start(), calls=%async_computation.8 | async-start | bytes 786432 | tf_op jit(solution)/shard_map/psum | solution.py:25
  22.1 2.2 copy-start.2
  25.6 79.7 %copy-start.5 = (bf16[64,128]{1,0:T(8,128)(2,1)S(1)}, bf16[64,128]{1,0:T(8,128)(2,1)}, u32[]{:S(2)}) copy-start(bf16[64,128]{1,0:T(8,128)(2,1)} %param.20) | copy-start | bytes 49156
  25.6 78.8 %reduce-scatter.7.cloned.1.call-start = ((), (), s32[]{:S(2)}) async-start(), calls=%async_computation.5 | async-start | bytes 294912
  69.8 59.0 %copy-start.7 = (f32[4096]{0:T(1024)S(1)}, f32[4096]{0:T(1024)}, u32[]{:S(2)}) copy-start(f32[4096]{0:T(1024)} %param.28) | copy-start | bytes 49156
  107.1 8.4 %all-to-all-start = ((bf16[4,2,1024]{2,1,0:T(2,128)(2,1)}), bf16[4,2,1024]{2,1,0:T(2,128)(2,1)S(1)}, u32[]{:S(2)}, u32[]{:S(2)}) async-start(bf16[4,2,1024]{2,1,0:T(2,128)(2,1)} %reshape.77), calls=%async_computation | async-start | bytes 32768 | tf_op jit(solution)/shard_map/all_to_all | solution.py:69
  110.8 97.1 %all-reduce.6.cloned.1.call-start = ((), (), s32[]{:S(2)}) async-start(), calls=%async_computation.4 | async-start | bytes 262144 | tf_op jit(solution)/shard_map/psum | solution.py:111
  128.8 0.6 copy-start.8
  132.6 4.8 %copy-start.9 = (f32[16]{0:T(128)S(1)}, f32[16]{0:T(128)}, u32[]{:S(2)}) copy-start(f32[16]{0:T(128)} %copy-done.8) | copy-start | bytes 196
  147.0 7.6 %copy-start.4 = (f32[16,2,256]{2,1,0:T(2,128)S(1)}, f32[16,2,256]{2,1,0:T(2,128)}, u32[]{:S(2)}) copy-start(f32[16,2,256]{2,1,0:T(2,128)} %reshape.63) | copy-start | bytes 98308
  148.7 6.0 %copy-start.1 = (bf16[512,4096]{1,0:T(8,128)(2,1)S(1)}, bf16[512,4096]{1,0:T(8,128)(2,1)}, u32[]{:S(2)}) copy-start(bf16[512,4096]{1,0:T(8,128)(2,1)} %param.35) | copy-start | bytes 12582916
  209.5 8.7 %all-to-all-start.1 = ((bf16[16,4,1024]{2,0,1:T(8,128)(2,1)}), bf16[16,4,1024]{2,0,1:T(8,128)(2,1)S(1)}, u32[]{:S(2)}, u32[]{:S(2)}) async-start(bf16[16,4,1024]{2,0,1:T(8,128)(2,1)} %bitcast.63), calls=%async_computation.1 | async-start | bytes 262144 | tf_op jit(solution)/shard_map/all_to_all | solution.py:113
  213.1 51.7 %all-reduce.8.cloned.1.call-start = ((), (), s32[]{:S(2)}) async-start(), calls=%async_computation.7 | async-start | bytes 786432 | tf_op jit(solution)/shard_map/psum | solution.py:25
  218.2 3.4 %copy-start.3 = (bf16[1024,1536]{1,0:T(8,128)(2,1)S(1)}, bf16[1024,1536]{1,0:T(8,128)(2,1)}, u32[]{:S(2)}) copy-start(bf16[1024,1536]{1,0:T(8,128)(2,1)} %param.37) | copy-start | bytes 9437188
  222.9 76.6 %reduce-scatter.9.cloned.1.call-start = ((), (), s32[]{:S(2)}) async-start(), calls=%async_computation.6 | async-start | bytes 294912
  268.5 4.2 %copy-start.6 = (f32[16,2,128]{2,1,0:T(2,128)S(1)}, f32[16,2,128]{2,1,0:T(2,128)}, u32[]{:S(2)}) copy-start(f32[16,2,128]{2,1,0:T(2,128)} %param.22) | copy-start | bytes 49156
Sparse Core Ops, SparseCore 0:
  25.7 44.0 all-reduce.9
  73.6 30.7 reduce-scatter.6
  156.2 51.6 all-reduce.5
  223.0 41.7 all-reduce.7
  268.6 30.7 reduce-scatter.8
where the time goes:
time: 308 us; the launch traced here: 307 us
  waiting for transfers between devices  185 us (60%)
  blocking collectives  46.2 us (15%)
  matrix products  30.2 us (10%)
  local copies, waits for them, and re-layouts  14 us (5%)
  between operations  13.9 us (5%)
  other arithmetic  10.6 us (3%)
  starting transfers between devices  7.45 us (2%)
    psum x2, waiting for transfers between devices, gated_block(): lax.psum(up_part.astype(jnp.bfloat16), 'kv').astype(jnp.float32)  67.2 us
    unnamed x7, waiting for transfers between devices  57 us
    psum x1, waiting for transfers between devices, body(): lax.psum(partial_heads.astype(jnp.bfloat16), 'tp').astype(jnp.float32)  51.8 us
    psum x2, blocking collectives, gated_block(): lax.psum(squares.astype(jnp.bfloat16), 'kv').astype(jnp.float32)  18.5 us
    all_gather x1, blocking collectives, body(): block = lax.all_gather(tokens, 'tp', axis=1, tiled=True)  14.9 us
    all_gather x1, blocking collectives, body(): lax.all_gather(moved, 'tp', axis=2, tiled=True)  12.8 us
  transfers between devices with their start and end apart: 7, of which 7 were waited for; matrix products, arithmetic and copies ran while one was open for 2% of the time, Pallas kernels for 0%

commit v1 on v0

--- a/solution.py
+++ b/solution.py
@@ -1,9 +1,12 @@
 import jax
 import jax.numpy as jnp
 from jax import lax
+from jax.experimental import pallas as pl
+from jax.experimental.pallas import tpu as pltpu
 from jax.sharding import PartitionSpec as P
 
 EPS = 1e-06
+MESH = pl.DeviceIdType.MESH
 
 
 def hidden_units(gate_acc, up_acc, squares, model_width):
@@ -119,6 +122,366 @@
     return (result, new_memory, new_normalizer, new_stabilizer)
 
 
+def tiles_fit(tokens, memory, first_down, kv_size, tp_size):
+    rows, col_width = tokens.shape
+    seqs, heads, value_size, key_size = memory.shape
+    hidden = first_down.shape[0]
+    return (
+        col_width % 128 == 0
+        and hidden % (128 * kv_size) == 0
+        and seqs % 16 == 0
+        and seqs * kv_size == rows
+        and key_size % 128 == 0
+        and value_size % 128 == 0
+        and tp_size > 1
+        and kv_size > 1
+    )
+
+
+def make_kernel(K, T, R, C, F, S, H, DK, DV):
+    f32, bf16 = jnp.float32, jnp.bfloat16
+    W, FQ = C * T, F // K
+    D = W * K
+    mlp_remote = 2 * (T - 1) + 3 * (K - 1)
+    remote_count = 2 * mlp_remote + 2 * (T - 1) + 2 * (K - 1)
+
+    def kernel(
+        tokens, normalizer, stabilizer, first_gain, mixer_gain, forget_bias, last_gain,
+        memory, fg, fu, fd, wq, wk, wv, wi, wf, wo, lg, lu, ld,
+        result, query_out, key_out, value_out, keep_out, admit_out, stab_out,
+        send_sem, recv_sem, load_sem,
+        v_fg, v_fu, v_fd, v_lg, v_lu, v_ld, v_qkv, v_wi, v_wf, v_wo, v_mem,
+        *bufs,
+    ):
+        mlp_bufs = (bufs[0:9], bufs[9:18])
+        s_one, moved, rows_all, rows_val, cell_in, qkv, cell_out, part, part_in, two, two_in, s_two = bufs[18:]
+        k = lax.axis_index("kv")
+        t = lax.axis_index("tp")
+        counter = [0]
+
+        loads = {}
+
+        def load(name, src, dst):
+            i = len(loads)
+            copy = pltpu.make_async_copy(src, dst, load_sem.at[i])
+            copy.start()
+            loads[name] = copy
+
+        load("fg", fg, v_fg)
+        load("fu", fu, v_fu)
+        load("fd", fd, v_fd)
+        load("wq", wq, v_qkv.at[:, pl.ds(0, H * DK)])
+        load("wk", wk, v_qkv.at[:, pl.ds(H * DK, H * DK)])
+        load("wv", wv, v_qkv.at[:, pl.ds(2 * H * DK, H * DV)])
+        load("wi", wi, v_wi)
+        load("wf", wf, v_wf)
+        load("mem", memory, v_mem)
+        load("wo", wo, v_wo)
+        load("lg", lg, v_lg)
+        load("lu", lu, v_lu)
+        load("ld", ld, v_ld)
+
+        barrier = pltpu.get_barrier_semaphore()
+        for o in range(1, T):
+            pl.semaphore_signal(barrier, inc=1, device_id=(k, lax.rem(t + o, T)), device_id_type=MESH)
+        for o in range(1, K):
+            pl.semaphore_signal(barrier, inc=1, device_id=(lax.rem(k + o, K), t), device_id_type=MESH)
+        pl.semaphore_wait(barrier, T + K - 2)
+
+        def send(src, dst, device):
+            i = counter[0]
+            counter[0] += 1
+            copy = pltpu.make_async_remote_copy(
+                src_ref=src, dst_ref=dst, send_sem=send_sem.at[i], recv_sem=recv_sem.at[i],
+                device_id=device, device_id_type=MESH,
+            )
+            copy.start()
+            return copy
+
+        started = []
+
+        def tp_to(o):
+            return (k, lax.rem(t + o, T))
+
+        def kv_to(o):
+            return (lax.rem(k + o, K), t)
+
+        def tp_from(o):
+            return lax.rem(t + (T - o), T)
+
+        def kv_from(o):
+            return lax.rem(k + (K - o), K)
+
+        def cols(at, width):
+            return pl.ds(pl.multiple_of(at * width, width), width)
+
+        def mlp(own, gain, vg, vu, vd, names, b):
+            gath, scaled, sq_out, sq_in, gu_out, gu_in, hid, hid_in, down = b[:9]
+            copies = [send(own, gath.at[o], tp_to(o)) for o in range(1, T)]
+            squares = jnp.zeros((R, C), f32)
+
+            def take(x, src, squares):
+                values = x.astype(f32)
+                at = pl.ds(pl.multiple_of((k * T + src) * C, C), C)
+                scaled[:, cols(src, C)] = (values * gain[:, at]).astype(bf16)
+                return squares + values * values
+
+            squares = take(own[...], t, squares)
+            for o in range(1, T):
+                copies[o - 1].wait_recv()
+                squares = take(gath[o], tp_from(o), squares)
+            started.extend(copies)
+            total = jnp.sum(squares, axis=1, keepdims=True)
+            sq_out[...] = jnp.broadcast_to(total, (R, 128))
+            sq_copies = [send(sq_out, sq_in.at[o], kv_to(o)) for o in range(1, K)]
+            loads[names[0]].wait()
+            loads[names[1]].wait()
+            x = scaled[...]
+            gu_copies = []
+            for o in range(1, K):
+                at = cols(lax.rem(k + o, K), FQ)
+                gu_out[o, 0] = jnp.dot(x, vg[:, at], preferred_element_type=f32).astype(bf16)
+                gu_out[o, 1] = jnp.dot(x, vu[:, at], preferred_element_type=f32).astype(bf16)
+                gu_copies.append(send(gu_out.at[o], gu_in.at[o], kv_to(o)))
+            at = cols(k, FQ)
+            gate = jnp.dot(x, vg[:, at], preferred_element_type=f32)
+            up = jnp.dot(x, vu[:, at], preferred_element_type=f32)
+            for c in sq_copies:
+                c.wait_recv()
+            for o in range(1, K):
+                total = total + sq_in[o][:, :1]
+            scale = lax.rsqrt(total / D + EPS)
+            for o in range(1, K):
+                gu_copies[o - 1].wait_recv()
+                gate = gate + gu_in[o, 0].astype(f32)
+                up = up + gu_in[o, 1].astype(f32)
+            gate = gate * scale
+            up = up * scale
+            mine = (gate / (1.0 + jnp.exp(-gate)) * up).astype(bf16)
+            hid_in[0] = mine
+            hid_copies = [send(hid_in.at[0], hid_in.at[o], kv_to(o)) for o in range(1, K)]
+            hid[:, cols(k, FQ)] = mine
+            loads[names[2]].wait()
+            for o in range(1, K):
+                hid_copies[o - 1].wait_recv()
+                hid[:, cols(kv_from(o), FQ)] = hid_in[o]
+            for c in range(0, T):
+                down[c] = jnp.dot(
+                    hid[...], vd[:, c * C:(c + 1) * C], preferred_element_type=f32
+                ).astype(bf16)
+            out_copies = [send(down.at[lax.rem(t + o, T)], gath.at[T + o], tp_to(o)) for o in range(1, T)]
+            acc = down[t].astype(f32)
+            for o in range(1, T):
+                out_copies[o - 1].wait_recv()
+                acc = acc + gath[T + o].astype(f32)
+            started.extend(sq_copies + gu_copies + hid_copies + out_copies)
+            return (own[...].astype(f32) + 0.5 * acc).astype(bf16)
+
+        s_one[...] = mlp(tokens, first_gain, v_fg, v_fu, v_fd, ("fg", "fu", "fd"), mlp_bufs[0])
+
+        move = [
+            send(s_one.at[pl.ds(pl.multiple_of(lax.rem(k + o, K) * S, S), S), :], moved.at[o], kv_to(o))
+            for o in range(1, K)
+        ]
+        moved[0] = s_one[pl.ds(pl.multiple_of(k * S, S), S), :]
+        for c in move:
+            c.wait_recv()
+        gather = [send(moved, rows_all.at[o], tp_to(o)) for o in range(1, T)]
+        squares = jnp.zeros((S, C), f32)
+        for o in range(0, T):
+            if o:
+                gather[o - 1].wait_recv()
+            for j in range(K):
+                values = (rows_all[o, j] if o else moved[j]).astype(f32)
+                at = cols(kv_from(j) * T + tp_from(o), C)
+                rows_val[:, at] = values
+                cell_in[:, at] = (values * mixer_gain[:, at]).astype(bf16)
+                squares = squares + values * values
+        started.extend(move + gather)
+        scale = lax.rsqrt(jnp.sum(squares, axis=1, keepdims=True) / D + EPS)
+        for name in ("wq", "wk", "wv", "wi", "wf"):
+            loads[name].wait()
+        width = 2 * H * DK + H * DV
+
+        def project(n, carry):
+            at = cols(n, 128 * 2 if width % 256 == 0 else 128)
+            qkv[:, at] = scale * jnp.dot(cell_in[...], v_qkv[:, at], preferred_element_type=f32)
+            return carry
+
+        lax.fori_loop(0, width // (256 if width % 256 == 0 else 128), project, 0)
+        input_all = scale * jnp.dot(cell_in[...], v_wi[...], preferred_element_type=f32)
+        forget_all = scale * jnp.dot(cell_in[...], v_wf[...], preferred_element_type=f32)
+        lane = lax.broadcasted_iota(jnp.int32, input_all.shape, 1)
+        loads["mem"].wait()
+        rowid = lax.broadcasted_iota(jnp.int32, (S, DV), 0)
+        query = qkv[:, : H * DK] * DK ** (-0.5)
+        key = qkv[:, H * DK : 2 * H * DK]
+        value = qkv[:, 2 * H * DK :]
+        query_out[...] = query
+        key_out[...] = key
+        value_out[...] = value
+        hi = query.astype(bf16)
+        lo = (query - hi.astype(f32)).astype(bf16)
+        dims = (((1,), (1,)), ((), ()))
+        step = 4 if S % 4 == 0 else 1
+
+        def recall(i, acc):
+            acc = list(acc)
+            for h in range(H):
+                qh = hi[:, h * DK : (h + 1) * DK]
+                ql = lo[:, h * DK : (h + 1) * DK]
+                for j in range(step):
+                    m = v_mem[i * step + j, h]
+                    mh = m.astype(bf16)
+                    ml = (m - mh.astype(f32)).astype(bf16)
+                    r = (
+                        lax.dot_general(qh, mh, dims, preferred_element_type=f32)
+                        + lax.dot_general(ql, mh, dims, preferred_element_type=f32)
+                        + lax.dot_general(qh, ml, dims, preferred_element_type=f32)
+                    )
+                    acc[h] = jnp.where(rowid == i * step + j, r, acc[h])
+            return tuple(acc)
+
+        recalled = lax.fori_loop(0, S // step, recall, tuple(jnp.zeros((S, DV), f32) for _ in range(H)))
+        for h in range(H):
+            own_head = lane == t * H + h
+            input_pre = jnp.sum(jnp.where(own_head, input_all, 0.0), axis=1, keepdims=True)
+            pre = jnp.sum(jnp.where(own_head, forget_all, 0.0), axis=1, keepdims=True) + forget_bias[:, h : h + 1]
+            log_forget = jnp.minimum(pre, 0.0) - jnp.log1p(jnp.exp(-jnp.abs(pre)))
+            carried = log_forget + stabilizer[:, h : h + 1]
+            new_stab = jnp.maximum(carried, input_pre)
+            keep = jnp.exp(carried - new_stab)
+            admit = jnp.exp(input_pre - new_stab)
+            stab_out[:, h : h + 1] = new_stab
+            keep_out[:, h : h + 1] = keep
+            admit_out[:, h : h + 1] = admit
+            qh = query[:, h * DK : (h + 1) * DK]
+            match = jnp.sum(qh * key[:, h * DK : (h + 1) * DK], axis=1, keepdims=True)
+            held = jnp.sum(qh * normalizer[:, h, :], axis=1, keepdims=True)
+            numer = keep * recalled[h] + (admit * match) * value[:, h * DV : (h + 1) * DV]
+            denom = keep * held + admit * match
+            cell_out[:, h * DV : (h + 1) * DV] = (numer / jnp.maximum(jnp.abs(denom), 1.0)).astype(bf16)
+
+        loads["wo"].wait()
+
+        def spread(j, carry):
+            for c in range(0, T):
+                at = pl.ds(pl.multiple_of(j * W + c * C, C), C)
+                part[c, j] = jnp.dot(cell_out[...], v_wo[:, at], preferred_element_type=f32).astype(bf16)
+            return carry
+
+        lax.fori_loop(0, K, spread, 0)
+        mix = [send(part.at[lax.rem(t + o, T)], part_in.at[o], tp_to(o)) for o in range(1, T)]
+        mixed = part[t].astype(f32)
+        for o in range(1, T):
+            mix[o - 1].wait_recv()
+            mixed = mixed + part_in[o].astype(f32)
+        for j in range(K):
+            at = cols(j * T + t, C)
+            two[j] = (rows_val[:, at] + mixed[j]).astype(bf16)
+        back = [send(two.at[lax.rem(k + o, K)], two_in.at[o], kv_to(o)) for o in range(1, K)]
+        s_two[pl.ds(pl.multiple_of(k * S, S), S), :] = two[k]
+        for o in range(1, K):
+            back[o - 1].wait_recv()
+            s_two[pl.ds(pl.multiple_of(kv_from(o) * S, S), S), :] = two_in[o]
+        started.extend(mix + back)
+
+        result[...] = mlp(s_two, last_gain, v_lg, v_lu, v_ld, ("lg", "lu", "ld"), mlp_bufs[1])
+        for c in started:
+            c.wait_send()
+
+    mlp_scratch = [
+        pltpu.VMEM((2 * T, R, C), bf16),
+        pltpu.VMEM((R, W), bf16),
+        pltpu.VMEM((R, 128), f32),
+        pltpu.VMEM((K, R, 128), f32),
+        pltpu.VMEM((K, 2, R, FQ), bf16),
+        pltpu.VMEM((K, 2, R, FQ), bf16),
+        pltpu.VMEM((R, F), bf16),
+        pltpu.VMEM((K, R, FQ), bf16),
+        pltpu.VMEM((T, R, C), bf16),
+    ]
+
+    def scratch(heads_all):
+        return [
+            pltpu.SemaphoreType.DMA((remote_count,)),
+            pltpu.SemaphoreType.DMA((remote_count,)),
+            pltpu.SemaphoreType.DMA((13,)),
+            pltpu.VMEM((W, F), bf16),
+            pltpu.VMEM((W, F), bf16),
+            pltpu.VMEM((F, W), bf16),
+            pltpu.VMEM((W, F), bf16),
+            pltpu.VMEM((W, F), bf16),
+            pltpu.VMEM((F, W), bf16),
+            pltpu.VMEM((D, 2 * H * DK + H * DV), bf16),
+            pltpu.VMEM((D, heads_all), bf16),
+            pltpu.VMEM((D, heads_all), bf16),
+            pltpu.VMEM((H * DV, D), bf16),
+            pltpu.VMEM((S, H, DV, DK), f32),
+            *mlp_scratch,
+            *mlp_scratch,
+            pltpu.VMEM((R, C), bf16),
+            pltpu.VMEM((K, S, C), bf16),
+            pltpu.VMEM((T, K, S, C), bf16),
+            pltpu.VMEM((S, D), f32),
+            pltpu.VMEM((S, D), bf16),
+            pltpu.VMEM((S, 2 * H * DK + H * DV), f32),
+            pltpu.VMEM((S, H * DV), bf16),
+            pltpu.VMEM((T, K, S, C), bf16),
+            pltpu.VMEM((T, K, S, C), bf16),
+            pltpu.VMEM((K, S, C), bf16),
+            pltpu.VMEM((K, S, C), bf16),
+            pltpu.VMEM((R, C), bf16),
+        ]
+
+    return kernel, scratch
+
+
+def fused_body(
+    tokens, memory, normalizer, stabilizer, first_gain, first_gate, first_up, first_down,
+    mixer_gain, query_weight, key_weight, value_weight, input_weight, forget_weight,
+    forget_bias, output_weight, last_gain, last_gate, last_up, last_down,
+):
+    f32 = jnp.float32
+    kv_size, tp_size = lax.axis_size("kv"), lax.axis_size("tp")
+    R, C = tokens.shape
+    S, H, DV, DK = memory.shape
+    F = first_down.shape[0]
+    kernel, scratch = make_kernel(kv_size, tp_size, R, C, F, S, H, DK, DV)
+    vmem, anyspace = pl.BlockSpec(memory_space=pltpu.VMEM), pl.BlockSpec(memory_space=pl.ANY)
+    shape = jax.ShapeDtypeStruct
+    result, query, key, value, keep, admit, new_stabilizer = pl.pallas_call(
+        kernel,
+        out_shape=(
+            shape((R, C), jnp.bfloat16),
+            shape((S, H * DK), f32),
+            shape((S, H * DK), f32),
+            shape((S, H * DV), f32),
+            shape((S, H), f32),
+            shape((S, H), f32),
+            shape((S, H), f32),
+        ),
+        in_specs=[vmem] * 7 + [anyspace] * 13,
+        out_specs=(vmem,) * 7,
+        scratch_shapes=scratch(input_weight.shape[1]),
+        compiler_params=pltpu.CompilerParams(
+            collective_id=0, has_side_effects=True, vmem_limit_bytes=60 * 2**20
+        ),
+    )(
+        tokens, normalizer, stabilizer, first_gain[None], mixer_gain[None], forget_bias[None], last_gain[None],
+        memory, first_gate, first_up, first_down, query_weight, key_weight, value_weight,
+        input_weight, forget_weight, output_weight, last_gate, last_up, last_down,
+    )
+    key = key.reshape(S, H, DK)
+    value = value.reshape(S, H, DV)
+    new_memory = (
+        keep[..., None, None] * memory
+        + admit[..., None, None] * value[..., :, None] * key[..., None, :]
+    )
+    new_normalizer = keep[..., None] * normalizer + admit[..., None] * key
+    return result, new_memory, new_normalizer, new_stabilizer
+
+
 def solution(mesh):
     in_specs = (
         P(None, ("kv", "tp")),
@@ -148,4 +511,10 @@
         P("kv", "tp", None),
         P("kv", "tp"),
     )
-    return jax.shard_map(body, mesh=mesh, in_specs=in_specs, out_specs=out_specs, check_vma=False)
+    kv_size, tp_size = mesh.shape["kv"], mesh.shape["tp"]
+
+    def chosen(tokens, memory, *rest):
+        fits = tiles_fit(tokens, memory, rest[5], kv_size, tp_size)
+        return (fused_body if fits else body)(tokens, memory, *rest)
+
+    return jax.shard_map(chosen, mesh=mesh, in_specs=in_specs, out_specs=out_specs, check_vma=False)

time: 308 us -> 86.8 us (0.28)
  waiting for transfers between devices: 185 us -> 0 us
  Pallas kernels: 0 us -> 71 us
  blocking collectives: 46.2 us -> 0 us
  matrix products: 30.2 us -> 0 us
  between operations: 13.9 us -> 0.7 us
  starting transfers between devices: 7.45 us -> 0 us
  local copies, waits for them, and re-layouts: 14 us -> 8.57 us
  other arithmetic: 10.6 us -> 6.04 us
    psum x3 -> x0, waiting for transfers between devices: 119 us -> none  [the longest x2 67.2 us: gated_block(): lax.psum(up_part.astype(jnp.bfloat16), 'kv').astype(jnp.float32)]
    pallas_call x0 -> x1, Pallas kernels: none -> 71 us  [fused_body(): pl.pallas_call(kernel, out_shape=(shape((R, C), jnp.bfloat16), shape((S,...]
    unnamed x7 -> x0, waiting for transfers between devices: 57 us -> none
    dot_general x13 -> x0, matrix products: 30.2 us -> none  [the longest x1 5.83 us: body(): jnp.einsum('bhvd,bhd->bhv', memory, query, precision=lax.Precision.HIGHEST)]
    all_gather x2 -> x0, blocking collectives: 27.7 us -> none  [the longest x1 14.9 us: body(): block = lax.all_gather(tokens, 'tp', axis=1, tiled=True)]
    psum x2 -> x0, blocking collectives: 18.5 us -> none  [gated_block(): lax.psum(squares.astype(jnp.bfloat16), 'kv').astype(jnp.float32)]
    all_to_all x2 -> x0, waiting for transfers between devices: 9.04 us -> none  [the longest x1 4.71 us: body(): lax.all_to_all(stream_one.reshape(rows, 1, col_width), 'kv', split_axis=0...]
    all_to_all x2 -> x0, starting transfers between devices: 7.32 us -> none  [the longest x1 3.67 us: body(): lax.all_to_all(stream_one.reshape(rows, 1, col_width), 'kv', split_axis=0...]
  transfers between devices with their start and end apart: 7 -> 0, of which waited for: 7 -> 0; matrix products, arithmetic and copies ran while one was open for 2% -> 0% of each run, Pallas kernels for 0% -> 0%
where the time goes in v1:
time: 86.8 us; the launch traced here: 86.3 us
  Pallas kernels  71 us (82%)
  local copies, waits for them, and re-layouts  8.57 us (10%)
  other arithmetic  6.04 us (7%)
    pallas_call x1, Pallas kernels, fused_body(): pl.pallas_call(kernel, out_shape=(shape((R, C), jnp.bfloat16), shape((S,...  71 us
    unnamed x15, local copies, waits for them, and re-layouts  7.06 us
    add x1, other arithmetic, fused_body(): keep[..., None, None] * memory  4.55 us

profile of v1, /device:TPU:0, one launch (start us, length us, event | category | flops | bytes accessed | tf_op | source)
XLA Modules:
  0.0 86.3 jit_solution(864204431535056801)
XLA Ops:
  0.6 2.2 %copy.25.wi = bf16[4096,16]{1,0:T(8,128)(2,1)} copy(bf16[4096,16]{0,1:T(8,128)(2,1)} %param.32) | data formatting | bytes 262144 | tf_op args[12]
  2.9 2.2 %copy.26.wf = bf16[4096,16]{1,0:T(8,128)(2,1)} copy(bf16[4096,16]{0,1:T(8,128)(2,1)} %param.33) | data formatting | bytes 262144 | tf_op args[13]
  5.1 1.4 %copy.24.stabilizer = f32[16,2]{1,0:T(8,128)} copy(f32[16,2]{0,1:T(2,128)} %param.23) | data formatting | bytes 256 | tf_op args[3]
  6.4 71.0 %shard_map.219 = (bf16[64,128]{1,0:T(8,128)(2,1)}, f32[16,256]{1,0:T(8,128)}, f32[16,256]{1,0:T(8,128)}, f32[16,512]{1,0:T(8,128)}, f32[16,2]{1,0:T(8,128)}, /*index=5*/f32[16,2]{1,0:T(8,128)}, f32[16,2]{1,0:T(8,128)}) custom-call(bf16[64,128]{1,0:T(8,128)(2,1)} %tokens.1, f32[16,2,128]{2,1,0:T(2,128)} %normalizer.1, f32[16,2]{1,0:T(8,128)} %copy.24.stabilizer, ...), custom_call_target="tpu_custom_call" | custom-call | tf_op jit(solution)/shard_map/pallas_call | solution.py:453
  77.5 0.8 broadcast_in_dim_reshape.4
  78.2 0.8 broadcast_multiply_fusion
  79.0 0.7 mul.57
  79.8 0.0 copy-start
  79.8 0.0 copy-start.1
  79.8 0.0 copy-start.2
  79.8 0.0 copy-start.4
  79.8 0.0 copy-start.3
  79.8 4.5 %multiply_add_fusion = f32[16,2,256,128]{3,2,1,0:T(8,128)} fusion(f32[16,2,256,128]{3,2,1,0:T(8,128)} %memory.1, f32[16,2,128]{2,1,0:T(2,128)S(1)} %mul.57, f32[16,2,256]{2,1,0:T(2,128)S(1)} %broadcast_multiply_fusion, f32[16,2]{1,0:T(8,128)} %get-tuple-element.11), kind=kLoop, calls=%fused_computation | loop fusion | flops 3145728 | bytes 8437888 | tf_op jit(solution)/shard_map/add | solution.py:478
  84.4 0.0 copy-done
  84.4 0.0 copy-done.1
  84.4 0.0 copy-done.2
  84.4 0.7 multiply_add_fusion.1
  85.1 0.0 copy-done.4
  85.1 0.6 copy.27
  85.7 0.0 copy-done.3
  85.7 0.6 copy.29
Async XLA Ops:
  79.8 4.6 %copy-start = (f32[16,2,128]{2,1,0:T(2,128)S(1)}, f32[16,2,128]{2,1,0:T(2,128)}, u32[]{:S(2)}) copy-start(f32[16,2,128]{2,1,0:T(2,128)} %normalizer.1) | copy-start | bytes 49156
  79.8 4.6 %copy-start.1 = (f32[16,2]{1,0:T(8,128)S(1)}, f32[16,2]{1,0:T(8,128)}, u32[]{:S(2)}) copy-start(f32[16,2]{1,0:T(8,128)} %get-tuple-element.11) | copy-start | bytes 388
  79.8 4.6 %copy-start.2 = (f32[16,2]{1,0:T(8,128)S(1)}, f32[16,2]{1,0:T(8,128)}, u32[]{:S(2)}) copy-start(f32[16,2]{1,0:T(8,128)} %get-tuple-element.12) | copy-start | bytes 388
  79.8 5.3 %copy-start.4 = (f32[16,2]{1,0:T(8,128)S(1)}, f32[16,2]{1,0:T(8,128)}, u32[]{:S(2)}) copy-start(f32[16,2]{1,0:T(8,128)} %get-tuple-element.19) | copy-start | bytes 388
  79.8 5.9 %copy-start.3 = (bf16[64,128]{1,0:T(8,128)(2,1)S(1)}, bf16[64,128]{1,0:T(8,128)(2,1)}, u32[]{:S(2)}) copy-start(bf16[64,128]{1,0:T(8,128)(2,1)} %get-tuple-element.24) | copy-start | bytes 49156

commit v2 on v1

--- a/solution.py
+++ b/solution.py
@@ -138,23 +138,22 @@
     )
 
 
-def make_kernel(K, T, R, C, F, S, H, DK, DV):
+def make_kernel(K, T, R, C, F, S, H, DK, DV, heads_all):
     f32, bf16 = jnp.float32, jnp.bfloat16
     W, FQ = C * T, F // K
     D = W * K
-    mlp_remote = 2 * (T - 1) + 3 * (K - 1)
-    remote_count = 2 * mlp_remote + 2 * (T - 1) + 2 * (K - 1)
+    remote_count = 4 * (T - 1) + 6 * (K - 1) + 2 * (K * T - 1)
 
     def kernel(
         tokens, normalizer, stabilizer, first_gain, mixer_gain, forget_bias, last_gain,
         memory, fg, fu, fd, wq, wk, wv, wi, wf, wo, lg, lu, ld,
-        result, query_out, key_out, value_out, keep_out, admit_out, stab_out,
+        result, v_mem, norm_out, stab_out,
         send_sem, recv_sem, load_sem,
-        v_fg, v_fu, v_fd, v_lg, v_lu, v_ld, v_qkv, v_wi, v_wf, v_wo, v_mem,
+        v_fg, v_fu, v_fd, v_lg, v_lu, v_ld, v_qkv, v_wif, v_wo,
         *bufs,
     ):
         mlp_bufs = (bufs[0:9], bufs[9:18])
-        s_one, moved, rows_all, rows_val, cell_in, qkv, cell_out, part, part_in, two, two_in, s_two = bufs[18:]
+        s_one, rows_in, rows_val, cell_in, qkv, cell_out, part, part_in, two, two_in, s_two, keep_rows = bufs[18:]
         k = lax.axis_index("kv")
         t = lax.axis_index("tp")
         counter = [0]
@@ -173,8 +172,8 @@
         load("wq", wq, v_qkv.at[:, pl.ds(0, H * DK)])
         load("wk", wk, v_qkv.at[:, pl.ds(H * DK, H * DK)])
         load("wv", wv, v_qkv.at[:, pl.ds(2 * H * DK, H * DV)])
-        load("wi", wi, v_wi)
-        load("wf", wf, v_wf)
+        load("wi", wi, v_wif.at[pl.ds(0, heads_all), :])
+        load("wf", wf, v_wif.at[pl.ds(heads_all, heads_all), :])
         load("mem", memory, v_mem)
         load("wo", wo, v_wo)
         load("lg", lg, v_lg)
@@ -182,11 +181,11 @@
         load("ld", ld, v_ld)
 
         barrier = pltpu.get_barrier_semaphore()
-        for o in range(1, T):
-            pl.semaphore_signal(barrier, inc=1, device_id=(k, lax.rem(t + o, T)), device_id_type=MESH)
-        for o in range(1, K):
-            pl.semaphore_signal(barrier, inc=1, device_id=(lax.rem(k + o, K), t), device_id_type=MESH)
-        pl.semaphore_wait(barrier, T + K - 2)
+        others = [(a, b) for a in range(K) for b in range(T) if a or b]
+        for a, b in others:
+            device = (lax.rem(k + a, K), lax.rem(t + b, T))
+            pl.semaphore_signal(barrier, inc=1, device_id=device, device_id_type=MESH)
+        pl.semaphore_wait(barrier, K * T - 1)
 
         def send(src, dst, device):
             i = counter[0]
@@ -215,24 +214,49 @@
         def cols(at, width):
             return pl.ds(pl.multiple_of(at * width, width), width)
 
-        def mlp(own, gain, vg, vu, vd, names, b):
-            gath, scaled, sq_out, sq_in, gu_out, gu_in, hid, hid_in, down = b[:9]
-            copies = [send(own, gath.at[o], tp_to(o)) for o in range(1, T)]
-            squares = jnp.zeros((R, C), f32)
-
-            def take(x, src, squares):
-                values = x.astype(f32)
-                at = pl.ds(pl.multiple_of((k * T + src) * C, C), C)
-                scaled[:, cols(src, C)] = (values * gain[:, at]).astype(bf16)
-                return squares + values * values
-
-            squares = take(own[...], t, squares)
-            for o in range(1, T):
-                copies[o - 1].wait_recv()
-                squares = take(gath[o], tp_from(o), squares)
-            started.extend(copies)
-            total = jnp.sum(squares, axis=1, keepdims=True)
-            sq_out[...] = jnp.broadcast_to(total, (R, 128))
+        def exchange(piece, land):
+            return {
+                (a, b): send(
+                    piece(lax.rem(k + a, K)), land.at[a * T + b], (lax.rem(k + a, K), lax.rem(t + b, T))
+                )
+                for a, b in others
+            }
+
+        def gain_at(gain, src):
+            return gain[:, pl.ds(pl.multiple_of((k * T + src) * C, C), C)]
+
+        def mlp(own, gain, vg, vu, vd, names, b, arrived=None):
+            gath, scaled, sq_out, sq_in, gu_out, gu_in, hid_in, down_acc, down = b[:9]
+            if arrived is None:
+                copies = [send(own, gath.at[o], tp_to(o)) for o in range(1, T)]
+                squares = jnp.zeros((R, C), f32)
+                for o in range(0, T):
+                    if o:
+                        copies[o - 1].wait_recv()
+                    src = tp_from(o)
+                    values = (gath[o] if o else own[...]).astype(f32)
+                    scaled[:, cols(src, C)] = (values * gain_at(gain, src)).astype(bf16)
+                    squares = squares + values * values
+                started.extend(copies)
+                sq_out[...] = jnp.broadcast_to(jnp.sum(squares, axis=1, keepdims=True), (R, 128))
+            else:
+                first, land, copies = arrived
+                for a in range(K):
+                    row = pl.ds(pl.multiple_of(kv_from(a) * S, S), S)
+                    squares = jnp.zeros((S, C), f32)
+                    for o in range(T):
+                        if a or o:
+                            copies[a, o].wait_recv()
+                        piece = land[a * T + o] if a or o else first
+                        src = tp_from(o)
+                        values = piece.astype(f32)
+                        scaled[row, cols(src, C)] = (values * gain_at(gain, src)).astype(bf16)
+                        squares = squares + values * values
+                        if o == 0:
+                            own[row, :] = piece
+                    sq_out[row, :] = jnp.broadcast_to(jnp.sum(squares, axis=1, keepdims=True), (S, 128))
+                started.extend(copies.values())
+            total = sq_out[:, :1]
             sq_copies = [send(sq_out, sq_in.at[o], kv_to(o)) for o in range(1, K)]
             loads[names[0]].wait()
             loads[names[1]].wait()
@@ -260,15 +284,26 @@
             mine = (gate / (1.0 + jnp.exp(-gate)) * up).astype(bf16)
             hid_in[0] = mine
             hid_copies = [send(hid_in.at[0], hid_in.at[o], kv_to(o)) for o in range(1, K)]
-            hid[:, cols(k, FQ)] = mine
             loads[names[2]].wait()
-            for o in range(1, K):
-                hid_copies[o - 1].wait_recv()
-                hid[:, cols(kv_from(o), FQ)] = hid_in[o]
-            for c in range(0, T):
-                down[c] = jnp.dot(
-                    hid[...], vd[:, c * C:(c + 1) * C], preferred_element_type=f32
-                ).astype(bf16)
+            half = max(W // 2, 128)
+
+            def rows_of(src):
+                return pl.ds(pl.multiple_of(src * FQ, FQ), FQ)
+
+            for o in range(K - 1):
+                if o:
+                    hid_copies[o - 1].wait_recv()
+                row = rows_of(kv_from(o))
+                for c in range(0, W, half):
+                    term = jnp.dot(hid_in[o], vd[row, c:c + half], preferred_element_type=f32)
+                    down_acc[:, c:c + half] = term + down_acc[:, c:c + half] if o else term
+            hid_copies[K - 2].wait_recv()
+            row = rows_of(kv_from(K - 1))
+            out_copies = []
+            for c in range(0, W, half):
+                term = down_acc[:, c:c + half] + jnp.dot(hid_in[K - 1], vd[row, c:c + half], preferred_element_type=f32)
+                for i in range(half // C):
+                    down[c // C + i] = term[:, i * C:(i + 1) * C].astype(bf16)
             out_copies = [send(down.at[lax.rem(t + o, T)], gath.at[T + o], tp_to(o)) for o in range(1, T)]
             acc = down[t].astype(f32)
             for o in range(1, T):
@@ -279,25 +314,22 @@
 
         s_one[...] = mlp(tokens, first_gain, v_fg, v_fu, v_fd, ("fg", "fu", "fd"), mlp_bufs[0])
 
-        move = [
-            send(s_one.at[pl.ds(pl.multiple_of(lax.rem(k + o, K) * S, S), S), :], moved.at[o], kv_to(o))
-            for o in range(1, K)
-        ]
-        moved[0] = s_one[pl.ds(pl.multiple_of(k * S, S), S), :]
-        for c in move:
-            c.wait_recv()
-        gather = [send(moved, rows_all.at[o], tp_to(o)) for o in range(1, T)]
+        def rows_for(group):
+            return s_one.at[pl.ds(pl.multiple_of(group * S, S), S), :]
+
+        gather = exchange(rows_for, rows_in)
         squares = jnp.zeros((S, C), f32)
-        for o in range(0, T):
-            if o:
-                gather[o - 1].wait_recv()
-            for j in range(K):
-                values = (rows_all[o, j] if o else moved[j]).astype(f32)
-                at = cols(kv_from(j) * T + tp_from(o), C)
+        for a in range(K):
+            for o in range(T):
+                if a or o:
+                    gather[a, o].wait_recv()
+                piece = rows_in[a * T + o] if a or o else s_one[pl.ds(pl.multiple_of(k * S, S), S), :]
+                values = piece.astype(f32)
+                at = cols(kv_from(a) * T + tp_from(o), C)
                 rows_val[:, at] = values
                 cell_in[:, at] = (values * mixer_gain[:, at]).astype(bf16)
                 squares = squares + values * values
-        started.extend(move + gather)
+        started.extend(gather.values())
         scale = lax.rsqrt(jnp.sum(squares, axis=1, keepdims=True) / D + EPS)
         for name in ("wq", "wk", "wv", "wi", "wf"):
             loads[name].wait()
@@ -309,56 +341,58 @@
             return carry
 
         lax.fori_loop(0, width // (256 if width % 256 == 0 else 128), project, 0)
-        input_all = scale * jnp.dot(cell_in[...], v_wi[...], preferred_element_type=f32)
-        forget_all = scale * jnp.dot(cell_in[...], v_wf[...], preferred_element_type=f32)
-        lane = lax.broadcasted_iota(jnp.int32, input_all.shape, 1)
+        dims = (((1,), (1,)), ((), ()))
+        gates = scale * lax.dot_general(cell_in[...], v_wif[...], dims, preferred_element_type=f32)
+        lane = lax.broadcasted_iota(jnp.int32, gates.shape, 1)
         loads["mem"].wait()
         rowid = lax.broadcasted_iota(jnp.int32, (S, DV), 0)
         query = qkv[:, : H * DK] * DK ** (-0.5)
         key = qkv[:, H * DK : 2 * H * DK]
         value = qkv[:, 2 * H * DK :]
-        query_out[...] = query
-        key_out[...] = key
-        value_out[...] = value
         hi = query.astype(bf16)
         lo = (query - hi.astype(f32)).astype(bf16)
-        dims = (((1,), (1,)), ((), ()))
+        both = jnp.concatenate([hi, lo], axis=0)
         step = 4 if S % 4 == 0 else 1
 
         def recall(i, acc):
             acc = list(acc)
             for h in range(H):
-                qh = hi[:, h * DK : (h + 1) * DK]
-                ql = lo[:, h * DK : (h + 1) * DK]
                 for j in range(step):
-                    m = v_mem[i * step + j, h]
-                    mh = m.astype(bf16)
-                    ml = (m - mh.astype(f32)).astype(bf16)
-                    r = (
-                        lax.dot_general(qh, mh, dims, preferred_element_type=f32)
-                        + lax.dot_general(ql, mh, dims, preferred_element_type=f32)
-                        + lax.dot_general(qh, ml, dims, preferred_element_type=f32)
-                    )
-                    acc[h] = jnp.where(rowid == i * step + j, r, acc[h])
+                    m = v_mem[i * step + j, h].astype(bf16)
+                    r = lax.dot_general(both[:, h * DK : (h + 1) * DK], m, dims, preferred_element_type=f32)
+                    acc[h] = jnp.where(rowid == i * step + j, r[:S] + r[S:], acc[h])
             return tuple(acc)
 
         recalled = lax.fori_loop(0, S // step, recall, tuple(jnp.zeros((S, DV), f32) for _ in range(H)))
+        eye = lax.broadcasted_iota(jnp.int32, (S, S), 0) == lax.broadcasted_iota(jnp.int32, (S, S), 1)
+        outer = []
         for h in range(H):
-            own_head = lane == t * H + h
-            input_pre = jnp.sum(jnp.where(own_head, input_all, 0.0), axis=1, keepdims=True)
-            pre = jnp.sum(jnp.where(own_head, forget_all, 0.0), axis=1, keepdims=True) + forget_bias[:, h : h + 1]
+            at = t * H + h
+            input_pre = jnp.sum(jnp.where(lane == at, gates, 0.0), axis=1, keepdims=True)
+            pre = jnp.sum(jnp.where(lane == at + heads_all, gates, 0.0), axis=1, keepdims=True)
+            pre = pre + forget_bias[:, h : h + 1]
+            held_stab = jnp.sum(jnp.where(eye, stabilizer[h : h + 1, :], 0.0), axis=1, keepdims=True)
             log_forget = jnp.minimum(pre, 0.0) - jnp.log1p(jnp.exp(-jnp.abs(pre)))
-            carried = log_forget + stabilizer[:, h : h + 1]
+            carried = log_forget + held_stab
             new_stab = jnp.maximum(carried, input_pre)
             keep = jnp.exp(carried - new_stab)
             admit = jnp.exp(input_pre - new_stab)
-            stab_out[:, h : h + 1] = new_stab
-            keep_out[:, h : h + 1] = keep
-            admit_out[:, h : h + 1] = admit
+            stab_out[h : h + 1, :] = jnp.sum(jnp.where(eye, new_stab, 0.0), axis=0, keepdims=True)
+            keep_rows[h] = jnp.broadcast_to(keep, (S, DK))
             qh = query[:, h * DK : (h + 1) * DK]
-            match = jnp.sum(qh * key[:, h * DK : (h + 1) * DK], axis=1, keepdims=True)
-            held = jnp.sum(qh * normalizer[:, h, :], axis=1, keepdims=True)
-            numer = keep * recalled[h] + (admit * match) * value[:, h * DV : (h + 1) * DV]
+            kh = key[:, h * DK : (h + 1) * DK]
+            vh = value[:, h * DV : (h + 1) * DV]
+            old_norm = normalizer[:, h, :]
+            match = jnp.sum(qh * kh, axis=1, keepdims=True)
+            held = jnp.sum(qh * old_norm, axis=1, keepdims=True)
+            norm_out[:, h, :] = keep * old_norm + admit * kh
+            admitted = admit * vh
+            a_hi = admitted.astype(bf16).astype(f32)
+            k_hi = kh.astype(bf16).astype(f32)
+            left = jnp.concatenate([a_hi, admitted - a_hi, a_hi], axis=0).T.astype(bf16)
+            right = jnp.concatenate([k_hi, k_hi, kh - k_hi], axis=0)
+            outer.append((left, right))
+            numer = keep * recalled[h] + (admit * match) * vh
             denom = keep * held + admit * match
             cell_out[:, h * DV : (h + 1) * DV] = (numer / jnp.maximum(jnp.abs(denom), 1.0)).astype(bf16)
 
@@ -372,6 +406,18 @@
 
         lax.fori_loop(0, K, spread, 0)
         mix = [send(part.at[lax.rem(t + o, T)], part_in.at[o], tp_to(o)) for o in range(1, T)]
+        row3 = lax.rem(lax.broadcasted_iota(jnp.int32, (3 * S, DK), 0), S)
+
+        def update(i, carry):
+            for h in range(H):
+                left, right = outer[h]
+                for j in range(step):
+                    n = i * step + j
+                    term = jnp.dot(left, jnp.where(row3 == n, right, 0.0).astype(bf16), preferred_element_type=f32)
+                    v_mem[n, h] = keep_rows[h, pl.ds(n, 1), :] * v_mem[n, h] + term
+            return carry
+
+        lax.fori_loop(0, S // step, update, 0)
         mixed = part[t].astype(f32)
         for o in range(1, T):
             mix[o - 1].wait_recv()
@@ -379,14 +425,11 @@
         for j in range(K):
             at = cols(j * T + t, C)
             two[j] = (rows_val[:, at] + mixed[j]).astype(bf16)
-        back = [send(two.at[lax.rem(k + o, K)], two_in.at[o], kv_to(o)) for o in range(1, K)]
-        s_two[pl.ds(pl.multiple_of(k * S, S), S), :] = two[k]
-        for o in range(1, K):
-            back[o - 1].wait_recv()
-            s_two[pl.ds(pl.multiple_of(kv_from(o) * S, S), S), :] = two_in[o]
-        started.extend(mix + back)
-
-        result[...] = mlp(s_two, last_gain, v_lg, v_lu, v_ld, ("lg", "lu", "ld"), mlp_bufs[1])
+        back = exchange(lambda group: two.at[group], two_in)
+        started.extend(mix)
+        result[...] = mlp(
+            s_two, last_gain, v_lg, v_lu, v_ld, ("lg", "lu", "ld"), mlp_bufs[1], (two[k], two_in, back)
+        )
         for c in started:
             c.wait_send()
 
@@ -397,12 +440,12 @@
         pltpu.VMEM((K, R, 128), f32),
         pltpu.VMEM((K, 2, R, FQ), bf16),
         pltpu.VMEM((K, 2, R, FQ), bf16),
-        pltpu.VMEM((R, F), bf16),
         pltpu.VMEM((K, R, FQ), bf16),
+        pltpu.VMEM((R, W), f32),
         pltpu.VMEM((T, R, C), bf16),
     ]
 
-    def scratch(heads_all):
+    def scratch():
         return [
             pltpu.SemaphoreType.DMA((remote_count,)),
             pltpu.SemaphoreType.DMA((remote_count,)),
@@ -414,15 +457,12 @@
             pltpu.VMEM((W, F), bf16),
             pltpu.VMEM((F, W), bf16),
             pltpu.VMEM((D, 2 * H * DK + H * DV), bf16),
-            pltpu.VMEM((D, heads_all), bf16),
-            pltpu.VMEM((D, heads_all), bf16),
+            pltpu.VMEM((2 * heads_all, D), bf16),
             pltpu.VMEM((H * DV, D), bf16),
-            pltpu.VMEM((S, H, DV, DK), f32),
             *mlp_scratch,
             *mlp_scratch,
             pltpu.VMEM((R, C), bf16),
-            pltpu.VMEM((K, S, C), bf16),
-            pltpu.VMEM((T, K, S, C), bf16),
+            pltpu.VMEM((K * T, S, C), bf16),
             pltpu.VMEM((S, D), f32),
             pltpu.VMEM((S, D), bf16),
             pltpu.VMEM((S, 2 * H * DK + H * DV), f32),
@@ -430,8 +470,9 @@
             pltpu.VMEM((T, K, S, C), bf16),
             pltpu.VMEM((T, K, S, C), bf16),
             pltpu.VMEM((K, S, C), bf16),
-            pltpu.VMEM((K, S, C), bf16),
+            pltpu.VMEM((K * T, S, C), bf16),
             pltpu.VMEM((R, C), bf16),
+            pltpu.VMEM((H, S, DK), f32),
         ]
 
     return kernel, scratch
@@ -447,39 +488,31 @@
     R, C = tokens.shape
     S, H, DV, DK = memory.shape
     F = first_down.shape[0]
-    kernel, scratch = make_kernel(kv_size, tp_size, R, C, F, S, H, DK, DV)
+    kernel, scratch = make_kernel(
+        kv_size, tp_size, R, C, F, S, H, DK, DV, input_weight.shape[1]
+    )
     vmem, anyspace = pl.BlockSpec(memory_space=pltpu.VMEM), pl.BlockSpec(memory_space=pl.ANY)
     shape = jax.ShapeDtypeStruct
-    result, query, key, value, keep, admit, new_stabilizer = pl.pallas_call(
+    result, new_memory, new_normalizer, new_stabilizer = pl.pallas_call(
         kernel,
         out_shape=(
             shape((R, C), jnp.bfloat16),
-            shape((S, H * DK), f32),
-            shape((S, H * DK), f32),
-            shape((S, H * DV), f32),
-            shape((S, H), f32),
-            shape((S, H), f32),
-            shape((S, H), f32),
+            pltpu.VMEM((S, H, DV, DK), f32),
+            shape((S, H, DK), f32),
+            shape((H, S), f32),
         ),
         in_specs=[vmem] * 7 + [anyspace] * 13,
-        out_specs=(vmem,) * 7,
-        scratch_shapes=scratch(input_weight.shape[1]),
+        out_specs=(vmem,) * 4,
+        scratch_shapes=scratch(),
         compiler_params=pltpu.CompilerParams(
-            collective_id=0, has_side_effects=True, vmem_limit_bytes=60 * 2**20
+            collective_id=0, has_side_effects=True, vmem_limit_bytes=57 * 2**20
         ),
     )(
-        tokens, normalizer, stabilizer, first_gain[None], mixer_gain[None], forget_bias[None], last_gain[None],
+        tokens, normalizer, stabilizer.T, first_gain[None], mixer_gain[None], forget_bias[None], last_gain[None],
         memory, first_gate, first_up, first_down, query_weight, key_weight, value_weight,
-        input_weight, forget_weight, output_weight, last_gate, last_up, last_down,
-    )
-    key = key.reshape(S, H, DK)
-    value = value.reshape(S, H, DV)
-    new_memory = (
-        keep[..., None, None] * memory
-        + admit[..., None, None] * value[..., :, None] * key[..., None, :]
-    )
-    new_normalizer = keep[..., None] * normalizer + admit[..., None] * key
-    return result, new_memory, new_normalizer, new_stabilizer
+        input_weight.T, forget_weight.T, output_weight, last_gate, last_up, last_down,
+    )
+    return result, new_memory, new_normalizer, new_stabilizer.T
 
 
 def solution(mesh):

time: 86.8 us -> 73 us (0.84)
  other arithmetic: 6.04 us -> 0 us
  local copies, waits for them, and re-layouts: 8.57 us -> 3.8 us
  Pallas kernels: 71 us -> 68.2 us
    add x2 -> x0, other arithmetic: 5.26 us -> none  [the longest x1 4.55 us: fused_body(): keep[..., None, None] * memory]
    unnamed x15 -> x10, local copies, waits for them, and re-layouts: 7.06 us -> 3.8 us
    pallas_call x1, Pallas kernels: 71 us -> 68.2 us  [fused_body(): pl.pallas_call(kernel, out_shape=(shape((R, C), jnp.bfloat16), pltpu.VMEM...]
where the time goes in v2:
time: 73 us; the launch traced here: 72.7 us
  Pallas kernels  68.2 us (93%)
  local copies, waits for them, and re-layouts  3.8 us (5%)
    pallas_call x1, Pallas kernels, fused_body(): pl.pallas_call(kernel, out_shape=(shape((R, C), jnp.bfloat16), pltpu.VMEM...  68.2 us
    unnamed x10, local copies, waits for them, and re-layouts  3.8 us

profile of v2, /device:TPU:0, one launch (start us, length us, event | category | flops | bytes accessed | tf_op | source)
XLA Modules:
  0.0 72.7 jit_solution(15070431159572857117)
XLA Ops:
  0.6 68.2 %shard_map.219 = (bf16[64,128]{1,0:T(8,128)(2,1)}, f32[16,2,256,128]{3,2,1,0:T(8,128)S(1)}, f32[16,2,128]{2,1,0:T(2,128)}, f32[2,16]{1,0:T(2,128)}) custom-call(bf16[64,128]{1,0:T(8,128)(2,1)} %tokens.1, f32[16,2,128]{2,1,0:T(2,128)} %normalizer.1, f32[2,16]{1,0:T(2,128)} %bitcast.13, f32[1,4096]{1,0:T(1,128)} %bitcast.10, f32[1,4096]{1,0:T(1,128)} %bitcast.11, ...), custom_call_target="tpu_custom_call" | custom-call | tf_op jit(solution)/shard_map/pallas_call | solution.py:496
  68.9 0.0 copy-start.1
  68.9 0.0 copy-start
  68.9 0.0 copy-start.2
  68.9 2.0 %copy.28 = f32[16,2,256,128]{3,2,1,0:T(8,128)} copy(f32[16,2,256,128]{3,2,1,0:T(8,128)S(1)} %get-tuple-element.13) | data formatting | bytes 8388608
  70.9 0.0 copy-done.1
  70.9 0.6 copy.29
  71.5 0.0 copy-done
  71.5 0.6 copy.30
  72.1 0.0 copy-done.2
  72.1 0.6 copy.31
Async XLA Ops:
  68.9 2.0 %copy-start.1 = (bf16[64,128]{1,0:T(8,128)(2,1)S(1)}, bf16[64,128]{1,0:T(8,128)(2,1)}, u32[]{:S(2)}) copy-start(bf16[64,128]{1,0:T(8,128)(2,1)} %get-tuple-element.20) | copy-start | bytes 49156
  68.9 2.6 %copy-start = (f32[16,2,128]{2,1,0:T(2,128)S(1)}, f32[16,2,128]{2,1,0:T(2,128)}, u32[]{:S(2)}) copy-start(f32[16,2,128]{2,1,0:T(2,128)} %get-tuple-element.22) | copy-start | bytes 49156
  68.9 3.2 %copy-start.2 = (f32[2,16]{1,0:T(2,128)S(1)}, f32[2,16]{1,0:T(2,128)}, u32[]{:S(2)}) copy-start(f32[2,16]{1,0:T(2,128)} %get-tuple-element.11) | copy-start | bytes 388
